TPU v7x, 256 devices: a whole 4x4x8 slice. The times are simulated.
256 devices in a mesh: sp: 32 (over z, x), tp: 8 (over y, core).
Axes of the slice: x: 4, y: 4, z: 8, core: 2. Of those that a mesh axis runs over, the one named last changes fastest.
Arguments:
- features: bfloat16 [12288, 2048], P('sp', 'tp'), may hold values from -6 to 6
- norm_gain: float32 [2048], replicated, may hold values from 0.28 to 10
- w_query: bfloat16 [2048, 1024], P(None, 'tp'), may hold values from -0.125 to 0.125
- w_key: bfloat16 [2048, 512], P(None, 'tp'), may hold values from -0.125 to 0.125
- w_value: bfloat16 [2048, 512], P(None, 'tp'), may hold values from -0.125 to 0.125
- head_sinks: float32 [16], P('tp'), may hold values from 1 to 5
- w_query_latent: bfloat16 [2048, 512], replicated, may hold values from -0.125 to 0.125
- w_kv_latent: bfloat16 [2048, 512], replicated, may hold values from -0.125 to 0.125
- w_rope_key: bfloat16 [2048, 64], replicated, may hold values from -0.125 to 0.125
- query_latent_gain: float32 [512], replicated, may hold values from 0.28 to 10
- kv_latent_gain: float32 [512], replicated, may hold values from 0.28 to 10
- w_query_content: bfloat16 [512, 1024], P(None, 'tp'), may hold values from -0.25 to 0.25
- w_query_rotary: bfloat16 [512, 512], P(None, 'tp'), may hold values from -0.25 to 0.25
- w_key_up: bfloat16 [512, 1024], P(None, 'tp'), may hold values from -0.25 to 0.25
- w_value_up: bfloat16 [512, 1024], P(None, 'tp'), may hold values from -0.25 to 0.25
- w_branch_window: bfloat16 [1024, 2048], P('tp'), may hold values from -0.1875 to 0.1875
- w_branch_latent: bfloat16 [1024, 2048], P('tp'), may hold values from -0.1875 to 0.1875
- w_gate_window: bfloat16 [2048, 2048], P(None, 'tp'), may hold values from -0.125 to 0.125
- w_gate_latent: bfloat16 [2048, 2048], P(None, 'tp'), may hold values from -0.125 to 0.125
Outputs:
- mixed: bfloat16 [12288, 2048], P('sp', 'tp')
All inputs are finite; a program needn't handle non-finite values.
Results may differ from a plain program's by a relative error of at most 0.018.
The roundings to bfloat16 on the way count: a program that leaves them out, or rounds other values in their place, can miss the bound.
Values may be sent and summed in bfloat16 or wider, within the bound.
A program may use at most 128 MiB of HBM per device.

v0:
```python
import jax
import jax.numpy as jnp
from jax import lax
from jax.sharding import PartitionSpec as P

HEAD = 64
WINDOW = 128
NOPE = 128
ROPE = 64
VDIM = 128
EPS = 1e-06
THETA = 10000.0
NEGATIVE = -1e30


def copy_for_each(shard, axis):
    count = lax.axis_size(axis)
    return lax.all_to_all(
        jnp.broadcast_to(shard[None], (count, *shard.shape)), axis, 0, 0, tiled=True
    )


def in_order(parts, dim):
    shape = list(parts.shape[1:])
    shape[dim] *= parts.shape[0]
    return jnp.moveaxis(parts, 0, dim).reshape(shape)


def gathered_copies(shard, axis, dim):
    parts = copy_for_each(shard, axis)
    return in_order(parts, dim)


def from_behind(shard, axis, by):
    count = lax.axis_size(axis)
    pairs = [(i, i + by) for i in range(count) if 0 <= i + by < count]
    return lax.ppermute(shard, axis, pairs)


def in_one_piece(arrays, axis, dim, along):
    widths = [a.shape[along] for a in arrays]
    both = jnp.concatenate(arrays, axis=along)
    result = lax.all_gather(both, axis, axis=dim, tiled=True)
    return tuple(jnp.split(result, [sum(widths[:k]) for k in range(1, len(widths))], axis=along))


def rms_rows(float_rows, gain_vec):
    return (
        float_rows
        * lax.rsqrt(jnp.mean(float_rows * float_rows, axis=-1, keepdims=True) + EPS)
        * gain_vec
    )


def rotate(float_rows, positions):
    half_width = float_rows.shape[-1] // 2
    frequencies = THETA ** (-jnp.arange(half_width, dtype=jnp.float32) / half_width)
    angles = positions.astype(jnp.float32)[:, None] * frequencies
    target = (float_rows.shape[0],) + (1,) * (float_rows.ndim - 2) + (half_width,)
    cosine = jnp.cos(angles).reshape(target)
    sine_part = jnp.sin(angles).reshape(target)
    first_half = float_rows[..., :half_width]
    second_half = float_rows[..., half_width:]
    return jnp.concatenate(
        [
            first_half * cosine - second_half * sine_part,
            second_half * cosine + first_half * sine_part,
        ],
        axis=-1,
    )


def project(left, right):
    return jnp.dot(left, right, preferred_element_type=jnp.float32)


def window_attention(queries, key_ext, value_ext, sink_table, row_start):
    row_count = queries.shape[0]
    kv_heads = key_ext.shape[1] // HEAD
    group_size = queries.shape[1] // HEAD // kv_heads
    blocks = row_count // WINDOW
    query_blocks = queries.reshape(blocks, WINDOW, kv_heads, group_size, HEAD)

    def banded(table):
        table = table.reshape(blocks + 1, WINDOW, kv_heads, HEAD)
        return jnp.concatenate([table[:-1], table[1:]], axis=1)

    key_band = banded(key_ext)
    value_band = banded(value_ext)
    scores = jnp.einsum(
        "nqhgd,nkhd->nhgqk", query_blocks, key_band, preferred_element_type=jnp.float32
    ) * HEAD ** (-0.5)
    query_index = jnp.arange(WINDOW, dtype=jnp.int32)[:, None]
    key_index = jnp.arange(2 * WINDOW, dtype=jnp.int32)[None, :]
    offset = query_index + WINDOW - key_index
    key_position = (
        row_start + jnp.arange(blocks, dtype=jnp.int32)[:, None, None] * WINDOW + key_index - WINDOW
    )
    valid_mask = ((offset >= 0) & (offset < WINDOW) & (key_position >= 0))[:, None, None]
    scores = jnp.where(valid_mask, scores, NEGATIVE)
    sink_logit = sink_table.reshape(1, kv_heads, group_size, 1, 1)
    row_top = jnp.maximum(jnp.max(scores, axis=-1, keepdims=True), sink_logit)
    weights = jnp.where(valid_mask, jnp.exp(scores - row_top), 0.0)
    denominator = jnp.sum(weights, axis=-1, keepdims=True) + jnp.exp(sink_logit - row_top)
    probabilities = (weights / denominator).astype(jnp.bfloat16)
    attended = jnp.einsum(
        "nhgqk,nkhd->nqhgd", probabilities, value_band, preferred_element_type=jnp.float32
    )
    return attended.astype(jnp.bfloat16).reshape(row_count, kv_heads * group_size * HEAD)


def on_device(
    features,
    norm_gain,
    w_query,
    w_key,
    w_value,
    head_sinks,
    w_query_latent,
    w_kv_latent,
    w_rope_key,
    query_latent_gain,
    kv_latent_gain,
    w_query_content,
    w_query_rotary,
    w_key_up,
    w_value_up,
    w_branch_window,
    w_branch_latent,
    w_gate_window,
    w_gate_latent,
):
    tok_rows = features.shape[0]
    row_start = lax.axis_index("sp") * tok_rows
    row_end = row_start + tok_rows
    positions = row_start + jnp.arange(tok_rows, dtype=jnp.int32)
    gathered = gathered_copies(features, "tp", 1)
    normed = rms_rows(gathered.astype(jnp.float32), norm_gain).astype(jnp.bfloat16)
    query_rows = project(normed, w_query).astype(jnp.bfloat16)
    key_rows = project(normed, w_key).astype(jnp.bfloat16)
    value_rows = project(normed, w_value).astype(jnp.bfloat16)
    key_width = key_rows.shape[1]
    packed = jnp.concatenate([key_rows, value_rows], axis=1)
    tail_rows = from_behind(packed[tok_rows - WINDOW :], "sp", 1)
    extended = jnp.concatenate([tail_rows, packed], axis=0)
    window_out = window_attention(
        query_rows, extended[:, :key_width], extended[:, key_width:], head_sinks, row_start
    )
    latent_query = rms_rows(project(normed, w_query_latent), query_latent_gain).astype(jnp.bfloat16)
    latent_kv = rms_rows(project(normed, w_kv_latent), kv_latent_gain).astype(jnp.bfloat16)
    rope_rows = rotate(project(normed, w_rope_key), positions).astype(jnp.bfloat16)
    lat_heads = w_key_up.shape[1] // NOPE
    query_content = (
        project(latent_query, w_query_content)
        .astype(jnp.bfloat16)
        .reshape(tok_rows, lat_heads, NOPE)
    )
    query_rotary = rotate(
        project(latent_query, w_query_rotary).reshape(tok_rows, lat_heads, ROPE), positions
    ).astype(jnp.bfloat16)
    scale_factor = (NOPE + ROPE) ** (-0.5)

    def attend(running, piece_keys, piece_values, rope_piece):
        running_max, denominator, accumulated = running
        piece_rows = piece_keys.shape[0]
        scores = (
            jnp.einsum(
                "qhd,khd->hqk",
                query_content,
                piece_keys.reshape(piece_rows, lat_heads, NOPE),
                preferred_element_type=jnp.float32,
            )
            + jnp.einsum(
                "qhr,kr->hqk", query_rotary, rope_piece, preferred_element_type=jnp.float32
            )
        ) * scale_factor
        key_position = jnp.arange(piece_rows, dtype=jnp.int32)
        live_mask = key_position[None, :] <= positions[:, None]
        scores = jnp.where(live_mask, scores, NEGATIVE)
        new_max = jnp.maximum(running_max, jnp.max(scores, axis=-1))
        weights = jnp.where(live_mask, jnp.exp(scores - new_max[..., None]), 0.0)
        denominator = jnp.sum(weights, axis=-1)
        accumulated = jnp.einsum(
            "hqk,khd->hqd",
            weights.astype(jnp.bfloat16),
            piece_values.reshape(piece_rows, lat_heads, VDIM),
            preferred_element_type=jnp.float32,
        )
        return (new_max, denominator, accumulated)

    initial = (
        jnp.full((lat_heads, tok_rows), NEGATIVE, jnp.float32),
        jnp.zeros((lat_heads, tok_rows), jnp.float32),
        jnp.zeros((lat_heads, tok_rows, VDIM), jnp.float32),
    )
    own_keys = project(latent_kv, w_key_up).astype(jnp.bfloat16)
    own_values = project(latent_kv, w_value_up).astype(jnp.bfloat16)
    pieces = in_one_piece((own_keys, own_values, rope_rows), "sp", 0, 1)
    running = lax.cond(
        jnp.int32(0) < row_end,
        lambda current: attend(current, pieces[0], pieces[1], pieces[2]),
        lambda current: current,
        initial,
    )
    latent_out = jnp.transpose(running[2] / running[1][..., None], (1, 0, 2))
    latent_out = latent_out.reshape(tok_rows, lat_heads * VDIM).astype(jnp.bfloat16)
    all_window, all_latent = in_one_piece((window_out, latent_out), "tp", 1, 0)
    column_window, column_latent = (
        lax.all_to_all(w_branch_window, "tp", split_axis=1, concat_axis=0, tiled=True),
        lax.all_to_all(w_branch_latent, "tp", split_axis=1, concat_axis=0, tiled=True),
    )
    window_branch = project(all_window, column_window)
    latent_branch = project(all_latent, column_latent)
    window_gate = jax.nn.sigmoid(project(normed, w_gate_window))
    latent_gate = jax.nn.sigmoid(project(normed, w_gate_latent))
    return (window_gate * window_branch + latent_gate * latent_branch).astype(jnp.bfloat16)


def solution(mesh):
    return jax.shard_map(
        on_device,
        mesh=mesh,
        in_specs=(
            P("sp", "tp"),
            P(),
            P(None, "tp"),
            P(None, "tp"),
            P(None, "tp"),
            P("tp"),
            P(),
            P(),
            P(),
            P(),
            P(),
            P(None, "tp"),
            P(None, "tp"),
            P(None, "tp"),
            P(None, "tp"),
            P("tp", None),
            P("tp", None),
            P(None, "tp"),
            P(None, "tp"),
        ),
        out_specs=P("sp", "tp"),
        check_vma=False,
    )
```

profile of v0, /device:TPU:36, one launch (start us, length us, event | category | flops | bytes accessed | tf_op | source)
XLA Modules:
  0.0 250.7 jit_solution(12856816892344930347)
XLA Ops:
  6.5 1.2 copy.42
  7.8 0.0 copy-start.15
  7.8 1.3 broadcast_in_dim.36
  9.1 4.5 %all-to-all-start = ((bf16[8,384,256]{1,2,0:T(8,128)(2,1)}), bf16[8,384,256]{1,2,0:T(8,128)(2,1)}, u32[]{:S(2)}, u32[]{:S(2)}) async-start(bf16[8,384,256]{1,2,0:T(8,128)(2,1)} %broadcast_in_dim.36), calls=%async_computation | async-start | bytes 3145728 | tf_op jit(solution)/shard_map/all_to_all | solution.py:18
  13.5 0.0 all-gather.3.cloned.1.call-start
  13.6 21.6 %all-to-all-done = bf16[8,384,256]{1,2,0:T(8,128)(2,1)} async-done(((bf16[8,384,256]{1,2,0:T(8,128)(2,1)}), bf16[8,384,256]{1,2,0:T(8,128)(2,1)}, u32[]{:S(2)}, u32[]{:S(2)}) %all-to-all-start) | async-done | bytes 1572896 | tf_op jit(solution)/shard_map/all_to_all | solution.py:18
  35.2 1.8 multiply_reduce_fusion
  37.0 1.8 fusion.19
  38.9 0.0 copy-start.11
  38.9 0.0 copy-start.16
  38.9 0.0 copy-start.12
  38.9 0.0 copy-start.10
  38.9 1.1 multiply_reduce_fusion.2
  40.1 0.4 convolution_convert_fusion.2
  40.4 0.0 copy-start.9
  40.5 0.4 convolution_convert_fusion.1
  40.9 0.4 fusion.65
  41.2 0.3 fusion.57
  41.5 0.7 pad_maximum_fusion
  42.2 0.0 all-gather.3.cloned.1.call-update
  42.3 0.0 all-gather.5.cloned.1.call-start
  42.3 0.0 copy-start.19
  42.3 0.1 add_compare_fusion
  42.5 0.2 broadcast_and_fusion
  42.6 1.9 convolution_convert_fusion.5
  44.6 1.8 convolution_convert_fusion.6
  46.4 0.0 copy-start.14
  46.4 0.0 copy-start.17
  46.4 0.0 copy-start.13
  46.4 3.2 %collective-permute-start = (bf16[128,128]{0,1:T(8,128)(2,1)S(1)}, bf16[128,128]{0,1:T(8,128)(2,1)S(1)}, u32[]{:S(2)}, u32[]{:S(2)}) collective-permute-start(bf16[128,128]{0,1:T(8,128)(2,1)S(1)} %pad_maximum_fusion.6), channel_id=1, source_target_pairs={{0,8},{8,16},{16,24},{24,32},{32,40},{40,48},{48,56},{56,64},{64,7... | collective-permute-start | bytes 98312 | tf_op jit(solution)/shard_map/ppermute | solution.py:37
  49.7 1.1 multiply_reduce_fusion.1
  50.8 0.3 convolution_bitcast_fusion
  51.2 0.3 fusion.53
  51.4 0.3 convolution_convert_fusion
  51.8 0.6 convolution_convert_fusion.4
  52.5 0.1 reshape.352
  52.7 0.3 fusion.64
  53.1 0.1 broadcast_maximum_fusion.1
  53.1 0.2 fusion.33
  53.3 0.1 exponential_add_fusion
  53.4 0.3 fusion.30
  53.7 0.1 copy.50
  53.8 89.5 %all-gather.3.cloned.1.call-done = bf16[12288,320]{0,1:T(8,128)(2,1)} async-done(((bf16[384,320]{0,1:T(8,128)(2,1)}), bf16[12288,320]{0,1:T(8,128)(2,1)}) %all-gather.3.cloned.1.call-update) | async-done | bytes 7864336 | tf_op jit(solution)/shard_map/all_gather | solution.py:43
  143.3 59.5 %conditional.1 = (f32[1,384]{1,0:T(1,128)S(1)}, f32[1,384,128]{1,2,0:T(8,128)S(1)}) conditional(s32[]{:T(128)} %convert_element_type.97, () %tuple.13, (s32[]{:T(128)}, s32[384]{0:T(512)S(1)}, bf16[12288,320]{0,1:T(8,128)(2,1)}, bf16[384,128]{1,0:T(8,128)(2,1)S(1)}, bf16[384,1,64]{0,2,1:T(8,128)(2,1)S(1)}) %tuple.14), branch_computations={%region_5.6_spmd, %region_6.9_spmd} | conditional | flops 3081240576 | bytes 119901712 | solution.py:199
  143.3 11.6 %copy.51 = bf16[12288,320]{1,0:T(8,128)(2,1)} copy(bf16[12288,320]{0,1:T(8,128)(2,1)} %get-tuple-element.44) | data formatting | bytes 15728640 | tf_op jit(solution)/shard_map
  154.9 9.8 %fusion.9 = f32[384,12288]{1,0:T(8,128)} fusion(bf16[384,128]{1,0:T(8,128)(2,1)S(1)} %get-tuple-element.25, bf16[12288,320]{1,0:T(8,128)(2,1)} %copy.51), kind=kOutput, calls=%fused_computation.11 | convolution fusion | flops 1207959552 | bytes 22118400 | tf_op jit(solution)/shard_map/cond/branch_1_fun/qhd,khd->hqk/dot_general | solution.py:167
  164.7 16.8 %fusion.63 = (f32[384]{0:T(512)S(1)}, f32[1,384,12288]{2,1,0:T(8,128)}) fusion(bf16[384,1,64]{0,2,1:T(8,128)(2,1)S(1)} %get-tuple-element.27, bf16[12288,320]{1,0:T(8,128)(2,1)} %copy.51, f32[384,12288]{1,0:T(8,128)} %fusion.9, s32[384]{0:T(512)S(1)} %broadcast_add_fusion), kind=kOutput, calls=%fused_computation.111 | convolution fusion | flops 627572352 | bytes 40946688 | tf_op jit(solution)/shard_map/cond/branch_1_fun/qhr,kr->hqk/dot_general | solution.py:173
  181.5 10.2 %fusion.11 = f32[1,384,128]{1,2,0:T(8,128)S(1)} fusion(bf16[12288,320]{1,0:T(8,128)(2,1)} %copy.51, f32[1,384,12288]{2,1,0:T(8,128)} %get-tuple-element.49, f32[384]{0:T(512)S(1)} %broadcast_maximum_fusion, s32[384]{0:T(512)S(1)} %broadcast_add_fusion), kind=kOutput, calls=%fused_computation.13 | convolution fusion | flops 1226833920 | bytes 22219776 | tf_op jit(solution)/shard_map/cond/branch_1_fun/hqk,khd->hqd/dot_general | solution.py:183
  191.7 11.1 %fusion.3 = f32[384]{0:T(512)S(1)} fusion(f32[1,384,12288]{2,1,0:T(8,128)} %get-tuple-element.49, f32[384]{0:T(512)S(1)} %broadcast_maximum_fusion, s32[384]{0:T(512)S(1)} %broadcast_add_fusion), kind=kLoop, calls=%fused_computation.6 | loop fusion | flops 18873984 | bytes 18878976 | tf_op jit(solution)/shard_map/cond/branch_1_fun/reduce_sum | solution.py:182
  202.9 0.7 pad_maximum_fusion.1
  203.6 0.0 all-gather.5.cloned.1.call-update
  203.6 1.0 copy.55
  204.6 4.3 %all-to-all-start.2 = ((bf16[128,8,256]{0,2,1:T(8,128)(2,1)}), bf16[128,8,256]{0,2,1:T(8,128)(2,1)S(1)}, u32[]{:S(2)}, u32[]{:S(2)}) async-start(bf16[128,8,256]{0,2,1:T(8,128)(2,1)} %bitcast.24), calls=%async_computation.2 | async-start | bytes 1048576 | tf_op jit(solution)/shard_map/all_to_all | solution.py:210
  208.9 1.0 copy.53
  209.9 10.4 %all-to-all-done.2 = bf16[128,8,256]{0,2,1:T(8,128)(2,1)S(1)} async-done(((bf16[128,8,256]{0,2,1:T(8,128)(2,1)}), bf16[128,8,256]{0,2,1:T(8,128)(2,1)S(1)}, u32[]{:S(2)}, u32[]{:S(2)}) %all-to-all-start.2) | async-done | bytes 524320 | tf_op jit(solution)/shard_map/all_to_all | solution.py:210
  220.3 3.7 %all-to-all-start.1 = ((bf16[128,8,256]{0,2,1:T(8,128)(2,1)}), bf16[128,8,256]{0,2,1:T(8,128)(2,1)S(1)}, u32[]{:S(2)}, u32[]{:S(2)}) async-start(bf16[128,8,256]{0,2,1:T(8,128)(2,1)} %bitcast.21), calls=%async_computation.1 | async-start | bytes 1048576 | tf_op jit(solution)/shard_map/all_to_all | solution.py:209
  224.0 0.2 copy.56
  224.2 9.8 %all-to-all-done.1 = bf16[128,8,256]{0,2,1:T(8,128)(2,1)S(1)} async-done(((bf16[128,8,256]{0,2,1:T(8,128)(2,1)}), bf16[128,8,256]{0,2,1:T(8,128)(2,1)S(1)}, u32[]{:S(2)}, u32[]{:S(2)}) %all-to-all-start.1) | async-done | bytes 524320 | tf_op jit(solution)/shard_map/all_to_all | solution.py:209
  234.0 1.0 copy.54
  235.1 2.7 %fusion.28 = f32[384,256]{1,0:T(8,128)} fusion(bf16[384,2048]{0,1:T(8,128)(2,1)S(1)} %copy-done.3, bf16[2048,256]{1,0:T(8,128)(2,1)} %param.39), kind=kOutput, calls=%fused_computation.35 | convolution fusion | flops 402948096 | bytes 3014656 | tf_op jit(solution)/shard_map/dot_general | solution.py:74
  237.8 2.2 fusion.25
  240.0 0.0 all-gather.5.cloned.1.call-done
  240.0 1.6 convolution_multiply_fusion.1
  241.6 2.2 fusion.29
  (59 shorter events, 0.4 us)
Async XLA Ops:
  6.5 32.3 %copy-start = (bf16[2048,512]{1,0:T(8,128)(2,1)S(1)}, bf16[2048,512]{1,0:T(8,128)(2,1)}, u32[]{:S(2)}) copy-start(bf16[2048,512]{1,0:T(8,128)(2,1)} %param.28) | copy-start | bytes 6291460
  7.8 29.2 %copy-start.15 = (f32[2048]{0:T(1024)S(1)}, f32[2048]{0:T(1024)}, u32[]{:S(2)}) copy-start(f32[2048]{0:T(1024)} %param.22) | copy-start | bytes 24580
  9.1 26.1 %all-to-all-start = ((bf16[8,384,256]{1,2,0:T(8,128)(2,1)}), bf16[8,384,256]{1,2,0:T(8,128)(2,1)}, u32[]{:S(2)}, u32[]{:S(2)}) async-start(bf16[8,384,256]{1,2,0:T(8,128)(2,1)} %broadcast_in_dim.36), calls=%async_computation | async-start | bytes 3145728 | tf_op jit(solution)/shard_map/all_to_all | solution.py:18
  13.5 129.8 %all-gather.3.cloned.1.call-start = ((), (), s32[]{:S(2)}) async-start(), calls=%async_computation.3 | async-start | bytes 8110080 | tf_op jit(solution)/shard_map/all_gather | solution.py:43
  38.9 2.0 copy-start.2
  38.9 1.2 copy-start.11
  38.9 1.2 copy-start.16
  38.9 1.5 copy-start.12
  38.9 1.9 copy-start.10
  40.0 2.6 %copy-start.8 = (bf16[2048,64]{0,1:T(8,128)(2,1)S(1)}, bf16[2048,64]{0,1:T(8,128)(2,1)}, u32[]{:S(2)}) copy-start(bf16[2048,64]{0,1:T(8,128)(2,1)} %param.25) | copy-start | bytes 786436
  40.4 4.1 %copy-start.9 = (bf16[2048,64]{0,1:T(8,128)(2,1)S(1)}, bf16[2048,64]{0,1:T(8,128)(2,1)}, u32[]{:S(2)}) copy-start(bf16[2048,64]{0,1:T(8,128)(2,1)} %param.24) | copy-start | bytes 786436
  41.2 8.4 %copy-start.3 = (bf16[384,2048]{0,1:T(8,128)(2,1)S(1)}, bf16[384,2048]{0,1:T(8,128)(2,1)}, u32[]{:S(2)}) copy-start(bf16[384,2048]{0,1:T(8,128)(2,1)} %copy-done.2) | copy-start | bytes 4718596
  42.3 197.7 %all-gather.5.cloned.1.call-start = ((), (), s32[]{:S(2)}) async-start(), calls=%async_computation.4 | async-start | bytes 1769472 | tf_op jit(solution)/shard_map/all_gather | solution.py:43
  42.3 7.4 %copy-start.19 = (bf16[2048,512]{1,0:T(8,128)(2,1)S(1)}, bf16[2048,512]{1,0:T(8,128)(2,1)}, u32[]{:S(2)}) copy-start(bf16[2048,512]{1,0:T(8,128)(2,1)} %param.27) | copy-start | bytes 6291460
  46.4 4.4 %copy-start.14 = (bf16[512,64]{0,1:T(8,128)(2,1)S(1)}, bf16[512,64]{0,1:T(8,128)(2,1)}, u32[]{:S(2)}) copy-start(bf16[512,64]{0,1:T(8,128)(2,1)} %param.33) | copy-start | bytes 196612
  46.4 4.4 %copy-start.17 = (f32[512]{0:T(512)S(1)}, f32[512]{0:T(512)}, u32[]{:S(2)}) copy-start(f32[512]{0:T(512)} %param.30) | copy-start | bytes 6148
  46.4 5.0 %copy-start.13 = (bf16[512,128]{1,0:T(8,128)(2,1)S(1)}, bf16[512,128]{1,0:T(8,128)(2,1)}, u32[]{:S(2)}) copy-start(bf16[512,128]{1,0:T(8,128)(2,1)} %param.32) | copy-start | bytes 393220
  46.4 5.4 %copy-start.7 = (bf16[2048,128]{1,0:T(8,128)(2,1)S(1)}, bf16[2048,128]{1,0:T(8,128)(2,1)}, u32[]{:S(2)}) copy-start(bf16[2048,128]{1,0:T(8,128)(2,1)} %param.23) | copy-start | bytes 1572868
  46.4 6.2 %collective-permute-start = (bf16[128,128]{0,1:T(8,128)(2,1)S(1)}, bf16[128,128]{0,1:T(8,128)(2,1)S(1)}, u32[]{:S(2)}, u32[]{:S(2)}) collective-permute-start(bf16[128,128]{0,1:T(8,128)(2,1)S(1)} %pad_maximum_fusion.6), channel_id=1, source_target_pairs={{0,8},{8,16},{16,24},{24,32},{32,40},{40,48},{48,56},{56,64},{64,7... | collective-permute-start | bytes 98312 | tf_op jit(solution)/shard_map/ppermute | solution.py:37
  51.4 1.6 copy-start.18
  143.3 60.3 %copy-start.4 = (bf16[128,2048]{1,0:T(8,128)(2,1)S(1)}, bf16[128,2048]{1,0:T(8,128)(2,1)}, u32[]{:S(2)}) copy-start(bf16[128,2048]{1,0:T(8,128)(2,1)} %param.37) | copy-start | bytes 1572868
  202.8 6.1 %copy-start.5 = (bf16[128,2048]{1,0:T(8,128)(2,1)S(1)}, bf16[128,2048]{1,0:T(8,128)(2,1)}, u32[]{:S(2)}) copy-start(bf16[128,2048]{1,0:T(8,128)(2,1)} %param.36) | copy-start | bytes 1572868
  204.6 15.7 %all-to-all-start.2 = ((bf16[128,8,256]{0,2,1:T(8,128)(2,1)}), bf16[128,8,256]{0,2,1:T(8,128)(2,1)S(1)}, u32[]{:S(2)}, u32[]{:S(2)}) async-start(bf16[128,8,256]{0,2,1:T(8,128)(2,1)} %bitcast.24), calls=%async_computation.2 | async-start | bytes 1048576 | tf_op jit(solution)/shard_map/all_to_all | solution.py:210
  220.3 13.7 %all-to-all-start.1 = ((bf16[128,8,256]{0,2,1:T(8,128)(2,1)}), bf16[128,8,256]{0,2,1:T(8,128)(2,1)S(1)}, u32[]{:S(2)}, u32[]{:S(2)}) async-start(bf16[128,8,256]{0,2,1:T(8,128)(2,1)} %bitcast.21), calls=%async_computation.1 | async-start | bytes 1048576 | tf_op jit(solution)/shard_map/all_to_all | solution.py:209
  235.1 2.7 %copy-start.20 = (bf16[2048,256]{1,0:T(8,128)(2,1)S(1)}, bf16[2048,256]{1,0:T(8,128)(2,1)}, u32[]{:S(2)}) copy-start(bf16[2048,256]{1,0:T(8,128)(2,1)} %param.38) | copy-start | bytes 3145732
  237.8 3.9 %copy-start.6 = (bf16[8,128,256]{2,1,0:T(8,128)(2,1)S(1)}, bf16[8,128,256]{2,1,0:T(8,128)(2,1)}, u32[]{:S(2)}) copy-start(bf16[8,128,256]{2,1,0:T(8,128)(2,1)} %copy.54) | copy-start | bytes 1572868
  237.8 6.1 %copy-start.1 = (bf16[2048,512]{1,0:T(8,128)(2,1)S(1)}, bf16[2048,512]{1,0:T(8,128)(2,1)}, u32[]{:S(2)}) copy-start(bf16[2048,512]{1,0:T(8,128)(2,1)} %param.28) | copy-start | bytes 6291460
Sparse Core Ops, SparseCore 0:
  42.4 100.8 all-gather.2
  203.7 27.3 all-gather.4
where the time goes:
time: 252 us; the launch traced here: 251 us
  waiting for transfers between devices  131 us (52%)
  matrix products  54.4 us (22%)
  local copies, waits for them, and re-layouts  17.9 us (7%)
  other arithmetic  17.4 us (7%)
  starting transfers between devices  15.8 us (6%)
  between operations  14 us (6%)
    all_gather x2, waiting for transfers between devices, in_one_piece(): result = lax.all_gather(both, axis, axis=dim, tiled=True)  89.5 us
    all_to_all x1, waiting for transfers between devices, copy_for_each(): lax.all_to_all(jnp.broadcast_to(shard[None], (count, *shard.shape)), axis...  21.6 us
    dot_general x14, matrix products, project(): return jnp.dot(left, right, preferred_element_type=jnp.float32)  17 us
    dot_general x1, matrix products, attend(): jnp.einsum('qhr,kr->hqk', query_rotary, rope_piece, preferred_element_typ...  16.8 us
    another operation x2, local copies, waits for them, and re-layouts  11.7 us
    reduce_sum x1, other arithmetic, attend(): denominator = jnp.sum(weights, axis=-1)  11.1 us
    all_to_all x1, waiting for transfers between devices, on_device(): lax.all_to_all(w_branch_latent, 'tp', split_axis=1, concat_axis=0, tiled=...  10.4 us
    dot_general x1, matrix products, attend(): jnp.einsum('hqk,khd->hqd', weights.astype(jnp.bfloat16), piece_values.res...  10.2 us
  transfers between devices with their start and end apart: 6, of which 4 were waited for; matrix products, arithmetic and copies ran while one was open for 6% of the time, Pallas kernels for 0%

commit v1 on v0

--- a/solution.py
+++ b/solution.py
@@ -1,3 +1,4 @@
+import functools
 import jax
 import jax.numpy as jnp
 from jax import lax
@@ -11,6 +12,43 @@
 EPS = 1e-06
 THETA = 10000.0
 NEGATIVE = -1e30
+
+
+def samples_all_proceed(message, on_dim, field):
+    f_next = message.shape
+    view_out = message.reshape(
+        *f_next[:on_dim], field, f_next[on_dim] // field, *f_next[on_dim + 1 :]
+    )
+    piece_now = jnp.moveaxis(view_out, on_dim, 0)
+    return piece_now
+
+
+def _save_frames(z_in, dim_no):
+    z_in = jnp.moveaxis(z_in, 0, dim_no)
+    x_next = z_in.shape
+    then = z_in.reshape(
+        *x_next[:dim_no], x_next[dim_no] * x_next[dim_no + 1], *x_next[dim_no + 2 :]
+    )
+    return then
+
+
+def group_axis_part(field_in, mesh_name, block_here, in_array):
+    earlier = lax.axis_index(mesh_name)
+    formed = lax.axis_size(mesh_name)
+    current_block, y1 = (formed, earlier)
+    state_next = samples_all_proceed(field_in, block_here, current_block)
+    buffer = [state_next[y1]]
+    for nth in range(1, current_block):
+        carry = state_next[y1 ^ nth]
+        big = lax.ppermute(carry, mesh_name, [(j, j ^ nth) for j in range(current_block)])
+        buffer.append(big)
+    w1 = jnp.stack(buffer, 0)
+    state_next = w1[y1 ^ jnp.arange(current_block)]
+    even = _save_frames(state_next, in_array)
+    return even
+
+
+enter_thing_on = functools.partial(group_axis_part, mesh_name="tp", block_here=1, in_array=0)
 
 
 def copy_for_each(shard, axis):
@@ -207,7 +245,7 @@
     all_window, all_latent = in_one_piece((window_out, latent_out), "tp", 1, 0)
     column_window, column_latent = (
         lax.all_to_all(w_branch_window, "tp", split_axis=1, concat_axis=0, tiled=True),
-        lax.all_to_all(w_branch_latent, "tp", split_axis=1, concat_axis=0, tiled=True),
+        enter_thing_on(w_branch_latent),
     )
     window_branch = project(all_window, column_window)
     latent_branch = project(all_latent, column_latent)

time: 252 us -> 243 us (0.964)
  waiting for transfers between devices: 131 us -> 119 us
  starting transfers between devices: 15.8 us -> 20.2 us
    all_to_all x1 -> x0, waiting for transfers between devices: 10.4 us -> none  [on_device(): lax.all_to_all(w_branch_latent, 'tp', split_axis=1, concat_axis=0, tiled=...]
    all_to_all x1, waiting for transfers between devices: 9.8 us -> 0.01 us  [on_device(): lax.all_to_all(w_branch_window, 'tp', split_axis=1, concat_axis=0, tiled=...]
    ppermute x0 -> x7, starting transfers between devices: none -> 8.89 us  [group_axis_part(): lax.ppermute(carry, mesh_name, [(j, j ^ nth) for j in range(current_block)])]
    ppermute x0 -> x7, waiting for transfers between devices: none -> 4.84 us  [group_axis_part(): lax.ppermute(carry, mesh_name, [(j, j ^ nth) for j in range(current_block)])]
    all_to_all x1 -> x0, starting transfers between devices: 4.29 us -> none  [on_device(): lax.all_to_all(w_branch_latent, 'tp', split_axis=1, concat_axis=0, tiled=...]
    all_gather x2, waiting for transfers between devices: 89.5 us -> 92.2 us  [in_one_piece(): result = lax.all_gather(both, axis, axis=dim, tiled=True)]
    another operation x2 -> x12, local copies, waits for them, and re-layouts: 11.7 us -> 12.6 us
  transfers between devices with their start and end apart: 6 -> 12, of which waited for: 4 -> 6; matrix products, arithmetic and copies ran while one was open for 6% -> 31% of each run, Pallas kernels for 0% -> 0%
where the time goes in v1:
time: 243 us; the launch traced here: 240 us
  waiting for transfers between devices  119 us (49%)
  matrix products  52.3 us (22%)
  starting transfers between devices  20.2 us (8%)
  local copies, waits for them, and re-layouts  17.6 us (7%)
  other arithmetic  17.4 us (7%)
  between operations  14.2 us (6%)
    all_gather x2, waiting for transfers between devices, in_one_piece(): result = lax.all_gather(both, axis, axis=dim, tiled=True)  92.2 us
    all_to_all x1, waiting for transfers between devices, copy_for_each(): lax.all_to_all(jnp.broadcast_to(shard[None], (count, *shard.shape)), axis...  21.6 us
    dot_general x1, matrix products, attend(): jnp.einsum('qhr,kr->hqk', query_rotary, rope_piece, preferred_element_typ...  16.7 us
    dot_general x14, matrix products, project(): return jnp.dot(left, right, preferred_element_type=jnp.float32)  15 us
    another operation x11, local copies, waits for them, and re-layouts  12.6 us
    reduce_sum x1, other arithmetic, attend(): denominator = jnp.sum(weights, axis=-1)  11.1 us
    dot_general x1, matrix products, attend(): jnp.einsum('hqk,khd->hqd', weights.astype(jnp.bfloat16), piece_values.res...  10.2 us
    dot_general x1, matrix products, attend(): jnp.einsum('qhd,khd->hqk', query_content, piece_keys.reshape(piece_rows,...  9.75 us
  transfers between devices with their start and end apart: 12, of which 6 were waited for; matrix products, arithmetic and copies ran while one was open for 31% of the time, Pallas kernels for 0%

profile of v1, /device:TPU:36, one launch (start us, length us, event | category | flops | bytes accessed | tf_op | source)
XLA Modules:
  0.0 240.3 jit_solution(14132055040269838728)
XLA Ops:
  6.5 1.2 copy.42
  7.8 1.3 broadcast_in_dim.36
  9.1 4.5 %all-to-all-start = ((bf16[8,384,256]{1,2,0:T(8,128)(2,1)}), bf16[8,384,256]{1,2,0:T(8,128)(2,1)}, u32[]{:S(2)}, u32[]{:S(2)}) async-start(bf16[8,384,256]{1,2,0:T(8,128)(2,1)} %broadcast_in_dim.36), calls=%async_computation | async-start | bytes 3145728 | tf_op jit(solution)/shard_map/all_to_all | solution.py:56
  13.6 21.6 %all-to-all-done = bf16[8,384,256]{1,2,0:T(8,128)(2,1)} async-done(((bf16[8,384,256]{1,2,0:T(8,128)(2,1)}), bf16[8,384,256]{1,2,0:T(8,128)(2,1)}, u32[]{:S(2)}, u32[]{:S(2)}) %all-to-all-start) | async-done | bytes 1572896 | tf_op jit(solution)/shard_map/all_to_all | solution.py:56
  35.2 1.8 multiply_reduce_fusion
  37.0 1.8 fusion.19
  38.9 0.4 fusion.66
  39.3 1.1 multiply_reduce_fusion.2
  40.5 0.4 convolution_convert_fusion.1
  40.9 0.4 convolution_convert_fusion.2
  41.2 0.3 fusion.57
  41.5 0.7 pad_maximum_fusion
  42.3 1.0 copy.53
  43.3 3.5 %all-to-all-start.1 = ((bf16[128,8,256]{0,2,1:T(8,128)(2,1)}), bf16[128,8,256]{0,2,1:T(8,128)(2,1)S(1)}, u32[]{:S(2)}, u32[]{:S(2)}) async-start(bf16[128,8,256]{0,2,1:T(8,128)(2,1)} %bitcast.21), calls=%async_computation.1 | async-start | bytes 1048576 | tf_op jit(solution)/shard_map/all_to_all | solution.py:247
  46.9 0.3 copy.55
  47.2 0.1 add_compare_fusion
  47.3 0.2 broadcast_and_fusion
  47.5 0.4 convolution_convert_fusion.6
  47.9 1.3 convolution_convert_fusion.5
  49.3 3.2 %collective-permute-start = (bf16[128,128]{0,1:T(8,128)(2,1)S(1)}, bf16[128,128]{0,1:T(8,128)(2,1)S(1)}, u32[]{:S(2)}, u32[]{:S(2)}) collective-permute-start(bf16[128,128]{0,1:T(8,128)(2,1)S(1)} %pad_maximum_fusion.6), channel_id=1, source_target_pairs={{0,8},{8,16},{16,24},{24,32},{32,40},{40,48},{48,56},{56,64},{64,7... | collective-permute-start | bytes 98312 | tf_op jit(solution)/shard_map/ppermute | solution.py:75
  52.5 1.1 multiply_reduce_fusion.1
  53.6 0.3 convolution_bitcast_fusion
  54.0 0.3 fusion.53
  54.3 0.3 convolution_convert_fusion
  54.6 0.6 convolution_convert_fusion.4
  55.3 0.1 reshape.396
  55.6 0.3 fusion.65
  56.0 0.2 fusion.33
  56.2 0.1 exponential_add_fusion
  56.2 0.3 fusion.30
  56.6 0.1 copy.50
  56.7 86.6 %all-gather.3.cloned.1.call-done = bf16[12288,320]{0,1:T(8,128)(2,1)} async-done(((bf16[384,320]{0,1:T(8,128)(2,1)}), bf16[12288,320]{0,1:T(8,128)(2,1)}) %all-gather.3.cloned.1.call-update) | async-done | bytes 7864336 | tf_op jit(solution)/shard_map/all_gather | solution.py:81
  143.3 59.4 %conditional.1 = (f32[1,384]{1,0:T(1,128)S(1)}, f32[1,384,128]{1,2,0:T(8,128)S(1)}) conditional(s32[]{:T(128)} %convert_element_type.97, () %tuple.13, (s32[]{:T(128)}, s32[384]{0:T(512)S(1)}, bf16[12288,320]{0,1:T(8,128)(2,1)}, bf16[384,128]{1,0:T(8,128)(2,1)S(1)}, bf16[384,1,64]{0,2,1:T(8,128)(2,1)S(1)}) %tuple.14), branch_computations={%region_5.6_spmd, %region_6.9_spmd} | conditional | flops 3081240576 | bytes 119901712 | solution.py:237
  143.3 11.6 %copy.51 = bf16[12288,320]{1,0:T(8,128)(2,1)} copy(bf16[12288,320]{0,1:T(8,128)(2,1)} %get-tuple-element.44) | data formatting | bytes 15728640 | tf_op jit(solution)/shard_map
  154.9 9.7 %fusion.9 = f32[384,12288]{1,0:T(8,128)} fusion(bf16[384,128]{1,0:T(8,128)(2,1)S(1)} %get-tuple-element.25, bf16[12288,320]{1,0:T(8,128)(2,1)} %copy.51), kind=kOutput, calls=%fused_computation.12 | convolution fusion | flops 1207959552 | bytes 22118400 | tf_op jit(solution)/shard_map/cond/branch_1_fun/qhd,khd->hqk/dot_general | solution.py:205
  164.7 16.7 %fusion.64 = (f32[384]{0:T(512)S(1)}, f32[1,384,12288]{2,1,0:T(8,128)}) fusion(bf16[384,1,64]{0,2,1:T(8,128)(2,1)S(1)} %get-tuple-element.27, bf16[12288,320]{1,0:T(8,128)(2,1)} %copy.51, f32[384,12288]{1,0:T(8,128)} %fusion.9, s32[384]{0:T(512)S(1)} %broadcast_add_fusion), kind=kOutput, calls=%fused_computation.131 | convolution fusion | flops 627572352 | bytes 40946688 | tf_op jit(solution)/shard_map/cond/branch_1_fun/qhr,kr->hqk/dot_general | solution.py:211
  181.3 10.2 %fusion.11 = f32[1,384,128]{1,2,0:T(8,128)S(1)} fusion(bf16[12288,320]{1,0:T(8,128)(2,1)} %copy.51, f32[1,384,12288]{2,1,0:T(8,128)} %get-tuple-element.49, f32[384]{0:T(512)S(1)} %broadcast_maximum_fusion, s32[384]{0:T(512)S(1)} %broadcast_add_fusion), kind=kOutput, calls=%fused_computation.14 | convolution fusion | flops 1226833920 | bytes 22219776 | tf_op jit(solution)/shard_map/cond/branch_1_fun/hqk,khd->hqd/dot_general | solution.py:221
  191.6 11.1 %fusion.3 = f32[384]{0:T(512)S(1)} fusion(f32[1,384,12288]{2,1,0:T(8,128)} %get-tuple-element.49, f32[384]{0:T(512)S(1)} %broadcast_maximum_fusion, s32[384]{0:T(512)S(1)} %broadcast_add_fusion), kind=kLoop, calls=%fused_computation.7 | loop fusion | flops 18873984 | bytes 18878976 | tf_op jit(solution)/shard_map/cond/branch_1_fun/reduce_sum | solution.py:220
  202.7 0.7 pad_maximum_fusion.1
  203.5 0.1 copy.57
  203.6 0.1 collective-permute-start.1
  203.7 0.1 copy.58
  203.8 1.6 collective-permute-start.2
  205.4 0.1 copy.59
  205.5 0.4 collective-permute-start.3
  206.0 0.1 copy.60
  206.1 3.3 %collective-permute-start.4 = (bf16[128,256]{1,0:T(8,128)(2,1)S(1)}, bf16[128,256]{1,0:T(8,128)(2,1)S(1)}, u32[]{:S(2)}, u32[]{:S(2)}) collective-permute-start(bf16[128,256]{1,0:T(8,128)(2,1)S(1)} %bitcast.138), channel_id=1, source_target_pairs={{0,4},{1,5},{2,6},{3,7},{4,0},{5,1},{6,2},{7,3},{8,12},{9,13},{10,... | collective-permute-start | bytes 196616 | tf_op jit(solution)/shard_map/ppermute | solution.py:43
  209.4 0.1 copy.61
  209.5 0.2 collective-permute-start.5
  209.7 0.1 copy.63
  209.9 0.1 copy.62
  210.0 0.1 copy.56
  210.1 2.8 %collective-permute-start.6 = (bf16[128,256]{1,0:T(8,128)(2,1)S(1)}, bf16[128,256]{1,0:T(8,128)(2,1)S(1)}, u32[]{:S(2)}, u32[]{:S(2)}) collective-permute-start(bf16[128,256]{1,0:T(8,128)(2,1)S(1)} %bitcast.139), channel_id=1, source_target_pairs={{0,6},{1,7},{2,4},{3,5},{4,2},{5,3},{6,0},{7,1},{8,14},{9,15},{10,... | collective-permute-start | bytes 196616 | tf_op jit(solution)/shard_map/ppermute | solution.py:43
  213.0 0.4 collective-permute-start.7
  213.4 2.0 collective-permute-done.5
  215.4 1.5 collective-permute-done.6
  216.9 1.4 collective-permute-done.7
  218.3 0.6 gather_fusion
  218.9 0.2 copy.54
  219.1 1.9 fusion.27
  221.1 3.0 %fusion.25 = f32[384,256]{1,0:T(8,128)} fusion(bf16[384,2048]{0,1:T(8,128)(2,1)} %copy-done.2, bf16[2048,256]{1,0:T(8,128)(2,1)S(1)} %copy-done.18), kind=kOutput, calls=%fused_computation.33 | convolution fusion | flops 402948096 | bytes 3014656 | tf_op jit(solution)/shard_map/dot_general | solution.py:112
  224.1 5.5 %all-gather.5.cloned.1.call-done = bf16[768,1024]{0,1:T(8,128)(2,1)} async-done(((bf16[768,128]{0,1:T(8,128)(2,1)}), bf16[768,1024]{0,1:T(8,128)(2,1)}) %all-gather.5.cloned.1.call-update) | async-done | bytes 1572880 | tf_op jit(solution)/shard_map/all_gather | solution.py:81
  229.6 1.6 convolution_multiply_fusion.2
  231.2 2.2 fusion.29
  (86 shorter events, 0.7 us)
Async XLA Ops:
  6.5 32.7 %copy-start = (bf16[2048,512]{1,0:T(8,128)(2,1)S(1)}, bf16[2048,512]{1,0:T(8,128)(2,1)}, u32[]{:S(2)}) copy-start(bf16[2048,512]{1,0:T(8,128)(2,1)} %param.28) | copy-start | bytes 6291460
  7.8 29.2 %copy-start.13 = (f32[2048]{0:T(1024)S(1)}, f32[2048]{0:T(1024)}, u32[]{:S(2)}) copy-start(f32[2048]{0:T(1024)} %param.22) | copy-start | bytes 24580
  9.1 26.1 %all-to-all-start = ((bf16[8,384,256]{1,2,0:T(8,128)(2,1)}), bf16[8,384,256]{1,2,0:T(8,128)(2,1)}, u32[]{:S(2)}, u32[]{:S(2)}) async-start(bf16[8,384,256]{1,2,0:T(8,128)(2,1)} %broadcast_in_dim.36), calls=%async_computation | async-start | bytes 3145728 | tf_op jit(solution)/shard_map/all_to_all | solution.py:56
  13.5 25.3 %copy-start.8 = (bf16[2048,64]{0,1:T(8,128)(2,1)S(1)}, bf16[2048,64]{0,1:T(8,128)(2,1)}, u32[]{:S(2)}) copy-start(bf16[2048,64]{0,1:T(8,128)(2,1)} %param.29) | copy-start | bytes 786436
  13.5 129.8 %all-gather.3.cloned.1.call-start = ((), (), s32[]{:S(2)}) async-start(), calls=%async_computation.2 | async-start | bytes 8110080 | tf_op jit(solution)/shard_map/all_gather | solution.py:81
  38.9 1.5 copy-start.2
  39.3 1.2 copy-start.9
  39.3 1.2 copy-start.14
  39.3 1.6 copy-start.10
  39.3 3.0 %copy-start.4 = (bf16[128,2048]{1,0:T(8,128)(2,1)S(1)}, bf16[128,2048]{1,0:T(8,128)(2,1)}, u32[]{:S(2)}) copy-start(bf16[128,2048]{1,0:T(8,128)(2,1)} %param.36) | copy-start | bytes 1572868
  40.4 6.5 %copy-start.5 = (bf16[128,2048]{1,0:T(8,128)(2,1)S(1)}, bf16[128,2048]{1,0:T(8,128)(2,1)}, u32[]{:S(2)}) copy-start(bf16[128,2048]{1,0:T(8,128)(2,1)} %param.37) | copy-start | bytes 1572868
  40.4 7.1 %copy-start.3 = (bf16[384,2048]{0,1:T(8,128)(2,1)S(1)}, bf16[384,2048]{0,1:T(8,128)(2,1)}, u32[]{:S(2)}) copy-start(bf16[384,2048]{0,1:T(8,128)(2,1)} %copy-done.2) | copy-start | bytes 4718596
  40.5 7.1 %copy-start.7 = (bf16[2048,64]{0,1:T(8,128)(2,1)S(1)}, bf16[2048,64]{0,1:T(8,128)(2,1)}, u32[]{:S(2)}) copy-start(bf16[2048,64]{0,1:T(8,128)(2,1)} %param.24) | copy-start | bytes 786436
  43.3 175.6 %all-to-all-start.1 = ((bf16[128,8,256]{0,2,1:T(8,128)(2,1)}), bf16[128,8,256]{0,2,1:T(8,128)(2,1)S(1)}, u32[]{:S(2)}, u32[]{:S(2)}) async-start(bf16[128,8,256]{0,2,1:T(8,128)(2,1)} %bitcast.21), calls=%async_computation.1 | async-start | bytes 1048576 | tf_op jit(solution)/shard_map/all_to_all | solution.py:247
  46.8 182.8 %all-gather.5.cloned.1.call-start = ((), (), s32[]{:S(2)}) async-start(), calls=%async_computation.3 | async-start | bytes 1769472 | tf_op jit(solution)/shard_map/all_gather | solution.py:81
  47.2 5.3 %copy-start.17 = (bf16[2048,512]{1,0:T(8,128)(2,1)S(1)}, bf16[2048,512]{1,0:T(8,128)(2,1)}, u32[]{:S(2)}) copy-start(bf16[2048,512]{1,0:T(8,128)(2,1)} %param.27) | copy-start | bytes 6291460
  49.2 4.4 %copy-start.12 = (bf16[512,64]{0,1:T(8,128)(2,1)S(1)}, bf16[512,64]{0,1:T(8,128)(2,1)}, u32[]{:S(2)}) copy-start(bf16[512,64]{0,1:T(8,128)(2,1)} %param.33) | copy-start | bytes 196612
  49.2 4.4 %copy-start.15 = (f32[512]{0:T(512)S(1)}, f32[512]{0:T(512)}, u32[]{:S(2)}) copy-start(f32[512]{0:T(512)} %param.30) | copy-start | bytes 6148
  49.2 5.0 %copy-start.11 = (bf16[512,128]{1,0:T(8,128)(2,1)S(1)}, bf16[512,128]{1,0:T(8,128)(2,1)}, u32[]{:S(2)}) copy-start(bf16[512,128]{1,0:T(8,128)(2,1)} %param.32) | copy-start | bytes 393220
  49.2 5.4 %copy-start.6 = (bf16[2048,128]{1,0:T(8,128)(2,1)S(1)}, bf16[2048,128]{1,0:T(8,128)(2,1)}, u32[]{:S(2)}) copy-start(bf16[2048,128]{1,0:T(8,128)(2,1)} %param.23) | copy-start | bytes 1572868
  49.3 6.2 %collective-permute-start = (bf16[128,128]{0,1:T(8,128)(2,1)S(1)}, bf16[128,128]{0,1:T(8,128)(2,1)S(1)}, u32[]{:S(2)}, u32[]{:S(2)}) collective-permute-start(bf16[128,128]{0,1:T(8,128)(2,1)S(1)} %pad_maximum_fusion.6), channel_id=1, source_target_pairs={{0,8},{8,16},{16,24},{24,32},{32,40},{40,48},{48,56},{56,64},{64,7... | collective-permute-start | bytes 98312 | tf_op jit(solution)/shard_map/ppermute | solution.py:75
  54.3 1.6 copy-start.16
  203.6 6.5 %collective-permute-start.1 = (bf16[128,256]{1,0:T(8,128)(2,1)S(1)}, bf16[128,256]{1,0:T(8,128)(2,1)S(1)}, u32[]{:S(2)}, u32[]{:S(2)}) collective-permute-start(bf16[128,256]{1,0:T(8,128)(2,1)S(1)} %bitcast.142), channel_id=1, source_target_pairs={{0,1},{1,0},{2,3},{3,2},{4,5},{5,4},{6,7},{7,6},{8,9},{9,8},{10,11... | collective-permute-start | bytes 196616 | tf_op jit(solution)/shard_map/ppermute | solution.py:43
  203.8 9.1 %collective-permute-start.2 = (bf16[128,256]{1,0:T(8,128)(2,1)S(1)}, bf16[128,256]{1,0:T(8,128)(2,1)S(1)}, u32[]{:S(2)}, u32[]{:S(2)}) collective-permute-start(bf16[128,256]{1,0:T(8,128)(2,1)S(1)} %bitcast.141), channel_id=1, source_target_pairs={{0,2},{1,3},{2,0},{3,1},{4,6},{5,7},{6,4},{7,5},{8,10},{9,11},{10,... | collective-permute-start | bytes 196616 | tf_op jit(solution)/shard_map/ppermute | solution.py:43
  205.5 7.9 %collective-permute-start.3 = (bf16[128,256]{1,0:T(8,128)(2,1)S(1)}, bf16[128,256]{1,0:T(8,128)(2,1)S(1)}, u32[]{:S(2)}, u32[]{:S(2)}) collective-permute-start(bf16[128,256]{1,0:T(8,128)(2,1)S(1)} %bitcast.140), channel_id=1, source_target_pairs={{0,3},{1,2},{2,1},{3,0},{4,7},{5,6},{6,5},{7,4},{8,11},{9,10},{10,... | collective-permute-start | bytes 196616 | tf_op jit(solution)/shard_map/ppermute | solution.py:43
  206.1 7.3 %collective-permute-start.4 = (bf16[128,256]{1,0:T(8,128)(2,1)S(1)}, bf16[128,256]{1,0:T(8,128)(2,1)S(1)}, u32[]{:S(2)}, u32[]{:S(2)}) collective-permute-start(bf16[128,256]{1,0:T(8,128)(2,1)S(1)} %bitcast.138), channel_id=1, source_target_pairs={{0,4},{1,5},{2,6},{3,7},{4,0},{5,1},{6,2},{7,3},{8,12},{9,13},{10,... | collective-permute-start | bytes 196616 | tf_op jit(solution)/shard_map/ppermute | solution.py:43
  209.5 5.9 %collective-permute-start.5 = (bf16[128,256]{1,0:T(8,128)(2,1)S(1)}, bf16[128,256]{1,0:T(8,128)(2,1)S(1)}, u32[]{:S(2)}, u32[]{:S(2)}) collective-permute-start(bf16[128,256]{1,0:T(8,128)(2,1)S(1)} %bitcast.137), channel_id=1, source_target_pairs={{0,5},{1,4},{2,7},{3,6},{4,1},{5,0},{6,3},{7,2},{8,13},{9,12},{10,... | collective-permute-start | bytes 196616 | tf_op jit(solution)/shard_map/ppermute | solution.py:43
  210.1 6.8 %collective-permute-start.6 = (bf16[128,256]{1,0:T(8,128)(2,1)S(1)}, bf16[128,256]{1,0:T(8,128)(2,1)S(1)}, u32[]{:S(2)}, u32[]{:S(2)}) collective-permute-start(bf16[128,256]{1,0:T(8,128)(2,1)S(1)} %bitcast.139), channel_id=1, source_target_pairs={{0,6},{1,7},{2,4},{3,5},{4,2},{5,3},{6,0},{7,1},{8,14},{9,15},{10,... | collective-permute-start | bytes 196616 | tf_op jit(solution)/shard_map/ppermute | solution.py:43
  213.0 5.3 %collective-permute-start.7 = (bf16[128,256]{1,0:T(8,128)(2,1)S(1)}, bf16[128,256]{1,0:T(8,128)(2,1)S(1)}, u32[]{:S(2)}, u32[]{:S(2)}) collective-permute-start(bf16[128,256]{1,0:T(8,128)(2,1)S(1)} %bitcast.136), channel_id=1, source_target_pairs={{0,7},{1,6},{2,5},{3,4},{4,3},{5,2},{6,1},{7,0},{8,15},{9,14},{10,... | collective-permute-start | bytes 196616 | tf_op jit(solution)/shard_map/ppermute | solution.py:43
  219.1 2.0 copy-start.18
  221.1 12.4 %copy-start.1 = (bf16[2048,512]{1,0:T(8,128)(2,1)S(1)}, bf16[2048,512]{1,0:T(8,128)(2,1)}, u32[]{:S(2)}) copy-start(bf16[2048,512]{1,0:T(8,128)(2,1)} %param.28) | copy-start | bytes 6291460
Sparse Core Ops, SparseCore 0:
  42.4 100.8 all-gather.2
  203.6 25.9 all-gather.4
